TPU v7x, 32 devices: a whole 2x2x4 slice. The times are simulated.
32 devices in a mesh: sp: 8 (over z, y), tp: 4 (over x, core).
Axes of the slice: x: 2, y: 2, z: 4, core: 2. Of those that a mesh axis runs over, the one named last changes fastest.
Arguments:
- queries: bfloat16 [8192, 1024], P('sp', 'tp'), may hold values from -6 to 6
- cell_key_rows: bfloat16 [8192, 1024], P('sp', 'tp'), may hold values from -6 to 6
- cell_value_rows: bfloat16 [8192, 2048], P('sp', 'tp'), may hold values from -6 to 6
- output_gate_logits: bfloat16 [8192, 2048], P('sp', 'tp'), may hold values from -6 to 6
- input_gate_logits: bfloat16 [8, 8192], P('tp', 'sp'), may hold values from -4 to 216
- forget_gate_logits: bfloat16 [8, 8192], P('tp', 'sp'), may hold values from 0.5 to 14
- forget_extra_term: float32 [8, 8192], P('tp', 'sp'), may hold values from -1.4 to 0
- residual: bfloat16 [8192, 2048], P('sp', 'tp'), may hold values from -13 to 13
- head_norm_gain: bfloat16 [2048], P('tp'), may hold values from 0.099609375 to 1.8984375
- cell_output_weight: bfloat16 [2048, 2048], P('tp'), may hold values from -0.25 to 0.25
- feedforward_norm_gain: bfloat16 [2048], replicated, may hold values from 0.099609375 to 1.8984375
- gate_projection_weight: bfloat16 [2048, 5632], P('sp', 'tp'), may hold values from -0.125 to 0.125
- up_projection_weight: bfloat16 [2048, 5632], P('sp', 'tp'), may hold values from -0.125 to 0.125
- down_projection_weight: bfloat16 [5632, 2048], P('tp', 'sp'), may hold values from -0.15625 to 0.15625
Outputs:
- mixed: bfloat16 [8192, 2048], P('sp', 'tp')
All inputs are finite; a program needn't handle non-finite values.
Results may differ from a plain program's by a relative error of at most 0.017.
Values may be sent and summed in bfloat16 or wider, within the bound.
A program may use at most 128 MiB of HBM per device.

v0:
```python
import jax
import jax.numpy as jnp
from jax import lax
from jax.sharding import PartitionSpec as P

PRECISE = lax.Precision.HIGHEST
LOWEST_LOG = -1e30
EPSILON = 1e-06


def entering(array, axis, combine, identity):
    length, index = (lax.axis_size(axis), lax.axis_index(axis))
    everything = jax.tree.map(lambda part: lax.all_gather(part, axis), array)
    start = jax.tree.map(
        lambda part, zero: jnp.broadcast_to(jnp.asarray(zero, part.dtype), part.shape),
        array,
        identity,
    )

    def step(k, before):
        reached = k < index
        new = combine(before, jax.tree.map(lambda part: part[k], everything))
        return jax.tree.map(lambda a, b: jnp.where(reached, a, b), new, before)

    return lax.fori_loop(0, length, step, start)


def to_blocks(array, block_count, block_size):
    shaped = array.reshape((array.shape[0], block_count, block_size) + array.shape[2:])
    return jnp.moveaxis(shaped, 1, 0)


def from_blocks(array):
    moved = jnp.moveaxis(array, 0, 1)
    return moved.reshape((moved.shape[0], moved.shape[1] * moved.shape[2]) + moved.shape[3:])


def memory_blocks(
    query_raw, key_raw, value_heads, in_gates, forget_log_value, block_size, query_scale
):
    head_count, length, key_width = query_raw.shape
    value_width = value_heads.shape[2]
    block_count = length // block_size
    causal = jnp.tril(jnp.ones((block_size, block_size), bool))

    def advance(carried, pieces):
        memory_state, top_log, offset = carried
        query_block, key_block, value_block, gate_block, forget_block = pieces
        running = jnp.cumsum(forget_block, axis=-1)
        log_weight = jnp.where(
            causal, running[:, :, None] - running[:, None, :] + gate_block[:, None, :], -jnp.inf
        )
        log_start = running + top_log[:, None]
        row_max = jnp.maximum(jnp.max(log_weight, axis=-1), log_start)
        scores = jnp.einsum(
            "htd,hsd->hts", query_block, key_block, preferred_element_type=jnp.float32
        )
        scores = scores * query_scale * jnp.exp(log_weight - row_max[:, :, None])
        query_wide = query_block.astype(jnp.float32) * query_scale
        earlier = jnp.einsum("htd,hde->hte", query_wide, memory_state, precision=PRECISE)
        numerator = jnp.exp(log_start - row_max)[:, :, None] * earlier
        numerator = numerator + jnp.einsum("hts,hse->hte", scores, value_block, precision=PRECISE)
        last_cum = running[:, -1]
        log_end = last_cum[:, None] - running + gate_block
        new_top = jnp.maximum(last_cum + top_log, jnp.max(log_end, axis=-1))
        scaled = key_block.astype(jnp.float32) * jnp.exp(log_end - new_top[:, None])[:, :, None]
        memory_state = jnp.exp(last_cum + top_log - new_top)[:, None, None] * memory_state
        memory_state = memory_state + jnp.einsum(
            "hsd,hse->hde", scaled, value_block, precision=PRECISE
        )
        return (
            (memory_state, new_top, offset + last_cum),
            (numerator, row_max, offset[:, None] + running),
        )

    initial = (
        jnp.zeros((head_count, key_width, value_width), jnp.float32),
        jnp.full((head_count,), LOWEST_LOG, jnp.float32),
        jnp.zeros((head_count,), jnp.float32),
    )
    pieces = tuple(
        (
            to_blocks(array, block_count, block_size)
            for array in (query_raw, key_raw, value_heads, in_gates, forget_log_value)
        )
    )
    ending, outputs = lax.scan(advance, initial, pieces)
    return (tuple((from_blocks(output) for output in outputs)), ending)


def join_states(earlier, later):
    state_early, top_early, total_early = earlier
    state_late, top_late, total_late = later
    moved_top = top_early + total_late
    new_top = jnp.maximum(moved_top, top_late)
    joined = jnp.exp(moved_top - new_top)[:, None, None] * state_early
    joined = joined + jnp.exp(top_late - new_top)[:, None, None] * state_late
    return (joined, new_top, total_early + total_late)


def heads_first(array, head_count):
    token_rows = array.shape[0]
    width = array.shape[1] // head_count
    return jnp.transpose(array.reshape(token_rows, head_count, width), (1, 0, 2))


def local(
    queries,
    cell_key_rows,
    cell_value_rows,
    output_gate_logits,
    input_gate_logits,
    forget_gate_logits,
    forget_extra_term,
    residual,
    head_norm_gain,
    cell_output_weight,
    feedforward_norm_gain,
    gate_projection_weight,
    up_projection_weight,
    down_projection_weight,
):
    whole_gate, whole_up, whole_down = (
        lax.all_gather(gate_projection_weight, "sp", axis=0, tiled=True),
        lax.all_gather(up_projection_weight, "sp", axis=0, tiled=True),
        lax.all_gather(down_projection_weight, "sp", axis=1, tiled=True),
    )
    token_rows = queries.shape[0]
    head_count = input_gate_logits.shape[0]
    key_width = queries.shape[1] // head_count
    value_width = cell_value_rows.shape[1] // head_count
    query_scale = key_width ** (-0.5)
    query_raw = heads_first(queries, head_count)
    key_raw = heads_first(cell_key_rows, head_count)
    value_heads = heads_first(cell_value_rows, head_count).astype(jnp.float32)
    forget_log_value = (
        jax.nn.log_sigmoid(forget_gate_logits.astype(jnp.float32)) + forget_extra_term
    )
    results, ending = memory_blocks(
        query_raw,
        key_raw,
        value_heads,
        input_gate_logits.astype(jnp.float32),
        forget_log_value,
        min(token_rows, 512),
        query_scale,
    )
    numerator, local_max, offsets = results
    end_state, end_top, end_total = ending
    identity = (
        jnp.zeros_like(end_state),
        jnp.full_like(end_top, LOWEST_LOG),
        jnp.zeros_like(end_total),
    )
    carried_state, carried_top, _ = entering(
        (end_state, end_top, end_total), "sp", join_states, identity
    )
    shifted = offsets + carried_top[:, None]
    row_max = jnp.maximum(local_max, shifted)
    query_heads = query_raw.astype(jnp.float32) * query_scale
    from_before = jnp.einsum("htd,hde->hte", query_heads, carried_state, precision=PRECISE)
    memory = (
        jnp.exp(local_max - row_max)[:, :, None] * numerator
        + jnp.exp(shifted - row_max)[:, :, None] * from_before
    )
    memory = jnp.transpose(memory, (1, 0, 2))
    normal = memory * lax.rsqrt(jnp.mean(memory * memory, axis=-1, keepdims=True) + EPSILON)
    gate_open = jax.nn.sigmoid(
        output_gate_logits.astype(jnp.float32).reshape(token_rows, head_count, value_width)
    )
    gated_heads = (
        normal * head_norm_gain.astype(jnp.float32).reshape(head_count, value_width) * gate_open
    )
    gated_heads = gated_heads.reshape(token_rows, head_count * value_width).astype(jnp.bfloat16)
    partial_value = jnp.dot(
        gated_heads, cell_output_weight, preferred_element_type=jnp.float32
    ).astype(jnp.bfloat16)
    column_count = residual.shape[1]
    column_start = lax.axis_index("tp") * column_count
    summed = lax.psum_scatter(partial_value, "tp", scatter_dimension=1, tiled=True).astype(
        jnp.float32
    )
    stream = (residual.astype(jnp.float32) + summed).astype(jnp.bfloat16)
    stream_local = stream.astype(jnp.float32)
    squares = lax.psum(jnp.sum(stream_local * stream_local, axis=1), "tp")
    scale = lax.rsqrt(squares / feedforward_norm_gain.shape[0] + EPSILON)[:, None]
    gain_columns = lax.dynamic_slice_in_dim(
        feedforward_norm_gain, column_start, column_count, 0
    ).astype(jnp.float32)
    normed = lax.all_gather(
        (stream_local * scale * gain_columns).astype(jnp.bfloat16), "tp", axis=1, tiled=True
    )
    gate_value = jnp.dot(normed, whole_gate, preferred_element_type=jnp.float32)
    lifted = jnp.dot(normed, whole_up, preferred_element_type=jnp.float32)
    hidden = (jax.nn.silu(gate_value) * lifted).astype(jnp.bfloat16)
    down_terms = jnp.dot(hidden, whole_down, preferred_element_type=jnp.float32)
    channel_total = lax.psum_scatter(
        down_terms.astype(jnp.bfloat16), "tp", scatter_dimension=1, tiled=True
    ).astype(jnp.float32)
    return (stream.astype(jnp.float32) + 0.5 * channel_total).astype(jnp.bfloat16)


def solution(mesh):
    placed = (
        P("sp", "tp"),
        P("sp", "tp"),
        P("sp", "tp"),
        P("sp", "tp"),
        P("tp", "sp"),
        P("tp", "sp"),
        P("tp", "sp"),
        P("sp", "tp"),
        P("tp"),
        P("tp", None),
        P(),
        P("sp", "tp"),
        P("sp", "tp"),
        P("tp", "sp"),
    )
    return jax.shard_map(
        local, mesh=mesh, in_specs=placed, out_specs=P("sp", "tp"), check_vma=False
    )
```

profile of v0, /device:TPU:0, one launch (start us, length us, event | category | flops | bytes accessed | tf_op | source)
XLA Modules:
  0.0 540.1 jit_solution(7199471552716918428)
XLA Ops:
  6.6 1.4 copy.44
  8.0 1.0 copy.45
  9.0 2.3 copy.42
  11.2 2.8 convert_bitcast_fusion
  14.1 2.9 copy.43
  17.0 1.3 copy.40
  18.3 0.3 copy.41
  18.6 18.4 %while.37 = (s32[]{:T(128)}, f32[2,128,256]{2,1,0:T(8,128)S(1)}, f32[2]{0:T(128)S(1)}, f32[2]{0:T(128)S(1)}, f32[2,2,512,256]{3,2,1,0:T(8,128)}, /*index=5*/f32[...) while((s32[]{:T(128)}, f32[2,128,256]{2,1,0:T(8,128)S(1)}, ...), condition=%wide.region_5.6_spmd.clone, body=%wide.region_0.5_spmd.clone.sunk | while | flops 2557093888 | bytes 39478384 | solution.py:87
  18.7 0.6 reduce-window.14
  19.5 0.2 reduce-window.15
  19.7 0.2 slice_reduce_fusion.5
  19.9 0.2 fusion.118
  20.2 0.7 fusion.121
  21.0 1.5 fusion.120
  22.5 2.6 fusion.122
  25.2 1.1 fusion.123
  26.4 1.3 convolution_add_fusion.2
  27.9 0.6 reduce-window.14
  28.9 0.2 slice_reduce_fusion.5
  29.1 0.2 fusion.118
  29.4 0.7 fusion.121
  30.1 1.5 fusion.120
  31.7 2.6 fusion.122
  34.4 1.1 fusion.123
  35.6 1.3 convolution_add_fusion.2
  37.0 0.7 copy-done.2
  37.8 0.6 dynamic-slice
  39.0 0.2 dynamic-update-slice
  39.3 0.2 dynamic-update-slice.1
  39.5 23.3 %all-reduce.2 = (f32[16]{0:T(128)S(1)}, f32[16]{0:T(128)S(1)}) all-reduce(f32[16]{0:T(128)S(1)} %dynamic-update-slice, f32[16]{0:T(128)S(1)} %dynamic-update-slice.1), channel_id=2, replica_groups=mesh['sp'=8,'tp'=4] {'sp'}, use_global_device_ids=true, to_apply=%add | all-reduce | flops 32 | bytes 256
  63.0 4.2 copy.49
  67.1 4.2 reshape.321
  71.3 1.9 add_divide_fusion
  73.2 2.9 copy.52
  76.1 13.6 %all-gather.17.cloned.1.call-done = f32[16,128,256]{2,1,0:T(8,128)} async-done(((f32[2,128,256]{2,1,0:T(8,128)}), f32[16,128,256]{2,1,0:T(8,128)}) %all-gather.17.cloned.1.call-update) | async-done | bytes 2097168 | tf_op jit(solution)/shard_map/all_gather | solution.py:13
  89.8 9.1 %while.38 = (s32[]{:T(128)}, f32[2,128,256]{2,1,0:T(8,128)S(1)}, f32[2]{0:T(128)S(1)}, s32[]{:T(128)}, f32[8,2]{1,0:T(8,128)S(1)}, /*index=5*/f32[8,2]{1,0:T(8,1...) while((s32[]{:T(128)}, f32[2,128,256]{2,1,0:T(8,128)S(1)}, f32[2]{0:T(128)S(1)}, s32[]{:T(128)}, ...), condition=%wide.region_7.8_spmd.clone, body=%wide.region_6.7_spmd.clone.sunk | while | flops 327698 | bytes 786647 | solution.py:25
  89.8 1.1 fusion.124
  91.0 1.1 fusion.124
  92.1 1.1 fusion.124
  93.3 1.1 fusion.124
  94.4 1.1 fusion.124
  95.5 1.1 fusion.124
  96.6 1.1 fusion.124
  97.8 1.1 fusion.124
  99.0 3.9 fusion.58
  102.9 0.3 fusion.61
  103.2 4.4 convolution_convert_fusion.1
  107.7 0.7 all-gather.11.cloned.1.call-update
  108.5 0.8 dynamic-slice_convert_fusion
  109.2 41.6 %reduce-scatter.3.cloned.1.call-done = bf16[1024,512]{1,0:T(8,128)(2,1)} async-done(((bf16[1024,2048]{1,0:T(8,128)(2,1)}), bf16[1024,512]{1,0:T(8,128)(2,1)}) %reduce-scatter.3.cloned.1.call-update) | async-done | bytes 1048592 | tf_op jit(solution)/shard_map/reduce_scatter | solution.py:180
  150.8 1.7 fusion.54
  152.5 5.8 %psum.7 = f32[1024]{0:T(1024)S(1)} all-reduce(f32[1024]{0:T(1024)S(1)} %fusion.54), channel_id=1, replica_groups=mesh['sp'=8,'tp'=4] {'tp'}, use_global_device_ids=true, to_apply=%region_11.12 | all-reduce | flops 1024 | bytes 8192 | tf_op jit(solution)/shard_map/psum | solution.py:185
  158.3 1.4 fusion.56
  159.7 0.5 all-gather.13.cloned.1.call-update
  160.3 0.5 all-gather.15.cloned.1.call-update
  160.9 0.3 reduce-scatter.5.cloned.1.call-start
  161.1 84.2 %all-gather.11.cloned.1.call-done = bf16[2048,1408]{1,0:T(8,128)(2,1)} async-done(((bf16[256,1408]{1,0:T(8,128)(2,1)}), bf16[2048,1408]{1,0:T(8,128)(2,1)}) %all-gather.11.cloned.1.call-update) | async-done | bytes 5767184 | tf_op jit(solution)/shard_map/all_gather | solution.py:124
  245.3 34.1 %all-gather.9.cloned.1.call-done = bf16[1024,2048]{1,0:T(8,128)(2,1)} async-done(((bf16[1024,512]{1,0:T(8,128)(2,1)}), bf16[1024,2048]{1,0:T(8,128)(2,1)}) %all-gather.9.cloned.1.call-update) | async-done | bytes 4194320 | tf_op jit(solution)/shard_map/all_gather | solution.py:190
  279.4 11.7 %fusion.74 = f32[1024,1408]{1,0:T(8,128)} fusion(bf16[1024,2048]{1,0:T(8,128)(2,1)} %all-gather.9.cloned.1.call-done, bf16[2048,1408]{1,0:T(8,128)(2,1)} %all-gather.11.cloned.1.call-done), kind=kOutput, calls=%fused_computation.117 | convolution fusion | flops 5905580032 | bytes 15728640 | tf_op jit(solution)/shard_map/dot_general | solution.py:193
  291.1 82.7 %all-gather.13.cloned.1.call-done = bf16[2048,1408]{1,0:T(8,128)(2,1)} async-done(((bf16[256,1408]{1,0:T(8,128)(2,1)}), bf16[2048,1408]{1,0:T(8,128)(2,1)}) %all-gather.13.cloned.1.call-update) | async-done | bytes 5767184 | tf_op jit(solution)/shard_map/all_gather | solution.py:125
  373.8 93.2 %all-gather.15.cloned.1.call-done = bf16[1408,2048]{1,0:T(8,128)(2,1)} async-done(((bf16[1408,256]{1,0:T(8,128)(2,1)}), bf16[1408,2048]{1,0:T(8,128)(2,1)}) %all-gather.15.cloned.1.call-update) | async-done | bytes 5767184 | tf_op jit(solution)/shard_map/all_gather | solution.py:126
  467.0 20.6 %convolution_convert_fusion = bf16[1024,2048]{1,0:T(8,128)(2,1)} fusion(bf16[1408,2048]{1,0:T(8,128)(2,1)} %all-gather.15.cloned.1.call-done, f32[1024,1408]{1,0:T(8,128)} %fusion.74, bf16[1024,2048]{1,0:T(8,128)(2,1)} %all-gather.9.cloned.1.call-done, bf16[2048,1408]{1,0:T(8,128)(2,1)} %all-gather.13.cloned.1.call-done), kind=kOutput, calls=%fused_computation.80 | convolution fusion | flops 11821907968 | bytes 25690112 | tf_op jit(solution)/shard_map/dot_general | solution.py:196
  487.6 42.7 %reduce-scatter.5.cloned.1.call-done = bf16[1024,512]{1,0:T(8,128)(2,1)} async-done(((bf16[1024,2048]{1,0:T(8,128)(2,1)}), bf16[1024,512]{1,0:T(8,128)(2,1)}) %reduce-scatter.5.cloned.1.call-update) | async-done | bytes 1048592 | tf_op jit(solution)/shard_map/reduce_scatter | solution.py:197
  530.3 3.0 fusion.57
  (114 shorter events, 2.6 us)
Async XLA Ops:
  6.5 96.7 %copy-start = (bf16[512,2048]{1,0:T(8,128)(2,1)S(1)}, bf16[512,2048]{1,0:T(8,128)(2,1)}, u32[]{:S(2)}) copy-start(bf16[512,2048]{1,0:T(8,128)(2,1)} %param.27) | copy-start | bytes 6291460
  6.5 83.2 %all-gather.17.cloned.1.call-start = ((), (), s32[]{:S(2)}) async-start(), calls=%async_computation.8 | async-start | bytes 2359296 | tf_op jit(solution)/shard_map/all_gather | solution.py:13
  8.0 6.1 %copy-start.8 = (bf16[1024,256]{0,1:T(8,128)(2,1)}, bf16[1024,256]{0,1:T(8,128)(2,1)S(1)}, u32[]{:S(2)}) copy-start(bf16[1024,256]{0,1:T(8,128)(2,1)S(1)} %copy.44) | copy-start | bytes 1572868
  17.0 1.6 copy-start.14
  17.0 1.6 copy-start.13
  17.0 1.6 copy-start.15
  18.6 19.2 %copy-start.17 = (u32[32]{0:T(128)S(1)}, u32[32]{0:T(128)}, u32[]{:S(2)}) copy-start(u32[32]{0:T(128)} %constant.100) | copy-start | bytes 388
  20.8 1.7 copy-start.3
  22.5 2.7 copy-start.4
  22.5 2.7 copy-start.10
  26.3 1.4 copy-start.11
  30.0 1.7 copy-start.3
  31.7 2.7 copy-start.4
  31.7 2.7 copy-start.10
  35.5 1.4 copy-start.11
  37.0 0.7 copy-start.2
  37.8 113.0 %reduce-scatter.3.cloned.1.call-start = ((), (), s32[]{:S(2)}) async-start(), calls=%async_computation.2 | async-start | bytes 5242880 | tf_op jit(solution)/shard_map/reduce_scatter | solution.py:180
  67.1 4.2 copy-start.12
  73.2 2.9 copy-start.16
  89.8 9.2 %copy-start.9 = (bf16[1024,256]{0,1:T(8,128)(2,1)S(1)}, bf16[1024,256]{0,1:T(8,128)(2,1)}, u32[]{:S(2)}) copy-start(bf16[1024,256]{0,1:T(8,128)(2,1)} %copy-done.8) | copy-start | bytes 1572868
  99.0 3.9 copy-start.7
  107.6 43.1 %copy-start.5 = (bf16[1024,512]{1,0:T(8,128)(2,1)S(1)}, bf16[1024,512]{1,0:T(8,128)(2,1)}, u32[]{:S(2)}) copy-start(bf16[1024,512]{1,0:T(8,128)(2,1)} %param.25) | copy-start | bytes 3145732
  107.7 137.6 %all-gather.11.cloned.1.call-start = ((), (), s32[]{:S(2)}) async-start(), calls=%async_computation.4 | async-start | bytes 6488064 | tf_op jit(solution)/shard_map/all_gather | solution.py:124
  108.4 171.0 %all-gather.9.cloned.1.call-start = ((), (), s32[]{:S(2)}) async-start(), calls=%async_computation.3 | async-start | bytes 5242880 | tf_op jit(solution)/shard_map/all_gather | solution.py:190
  150.8 7.5 %copy-start.6 = (bf16[1024,512]{1,0:T(8,128)(2,1)S(1)}, bf16[1024,512]{1,0:T(8,128)(2,1)}, u32[]{:S(2)}) copy-start(bf16[1024,512]{1,0:T(8,128)(2,1)} %reduce-scatter.3.cloned.1.call-done) | copy-start | bytes 3145732
  159.7 214.1 %all-gather.13.cloned.1.call-start = ((), (), s32[]{:S(2)}) async-start(), calls=%async_computation.5 | async-start | bytes 6488064 | tf_op jit(solution)/shard_map/all_gather | solution.py:125
  160.3 306.7 %all-gather.15.cloned.1.call-start = ((), (), s32[]{:S(2)}) async-start(), calls=%async_computation.6 | async-start | bytes 6488064 | tf_op jit(solution)/shard_map/all_gather | solution.py:126
  160.9 369.5 %reduce-scatter.5.cloned.1.call-start = ((), (), s32[]{:S(2)}) async-start(), calls=%async_computation.7 | async-start | bytes 5242880 | tf_op jit(solution)/shard_map/reduce_scatter | solution.py:197
  487.6 45.7 %copy-start.1 = (bf16[512,2048]{1,0:T(8,128)(2,1)S(1)}, bf16[512,2048]{1,0:T(8,128)(2,1)}, u32[]{:S(2)}) copy-start(bf16[512,2048]{1,0:T(8,128)(2,1)} %param.27) | copy-start | bytes 6291460
Sparse Core Ops, SparseCore 0:
  37.9 51.8 all-gather.16
  107.8 42.9 reduce-scatter.2
  153.0 92.2 all-gather.10
  246.7 32.6 all-gather.8
  281.4 92.3 all-gather.12
  375.7 91.3 all-gather.14
  487.7 42.5 reduce-scatter.4
where the time goes:
time: 541 us; the launch traced here: 540 us
  waiting for transfers between devices  394 us (73%)
  matrix products  53.6 us (10%)
  blocking collectives  29.1 us (5%)
  other arithmetic  25.1 us (5%)
  local copies, waits for them, and re-layouts  23.3 us (4%)
  between operations  14.3 us (3%)
    all_gather x1, waiting for transfers between devices, local(): lax.all_gather(down_projection_weight, 'sp', axis=1, tiled=True)  93.2 us
    all_gather x1, waiting for transfers between devices, local(): lax.all_gather(gate_projection_weight, 'sp', axis=0, tiled=True)  84.2 us
    all_gather x1, waiting for transfers between devices, local(): lax.all_gather(up_projection_weight, 'sp', axis=0, tiled=True)  82.7 us
    reduce_scatter x1, waiting for transfers between devices, local(): lax.psum_scatter(down_terms.astype(jnp.bfloat16), 'tp', scatter_dimension...  42.7 us
    reduce_scatter x1, waiting for transfers between devices, local(): lax.psum_scatter(partial_value, 'tp', scatter_dimension=1, tiled=True)  41.6 us
    all_gather x1, waiting for transfers between devices, local(): lax.all_gather((stream_local * scale * gain_columns).astype(jnp.bfloat16)...  34.1 us
    unnamed x1, blocking collectives  23.3 us
    dot_general x1, matrix products, local(): down_terms = jnp.dot(hidden, whole_down, preferred_element_type=jnp.float32)  20.6 us
  transfers between devices with their start and end apart: 7, of which 7 were waited for; matrix products, arithmetic and copies ran while one was open for 6% of the time, Pallas kernels for 0%

commit v1 on v0

--- a/solution.py
+++ b/solution.py
@@ -6,6 +6,16 @@
 PRECISE = lax.Precision.HIGHEST
 LOWEST_LOG = -1e30
 EPSILON = 1e-06
+
+
+def ring_gather(x, axis, dim):
+    ways, here, step = (lax.axis_size(axis), lax.axis_index(axis), x.shape[dim])
+    shape = [n * ways if d == dim else n for d, n in enumerate(x.shape)]
+    full = lax.dynamic_update_slice_in_dim(jnp.zeros(shape, x.dtype), x, here * step, axis=dim)
+    for far in range(1, ways):
+        x = lax.ppermute(x, axis, [(d, (d + 1) % ways) for d in range(ways)])
+        full = lax.dynamic_update_slice_in_dim(full, x, (here - far) % ways * step, axis=dim)
+    return full
 
 
 def entering(array, axis, combine, identity):
@@ -122,7 +132,7 @@
 ):
     whole_gate, whole_up, whole_down = (
         lax.all_gather(gate_projection_weight, "sp", axis=0, tiled=True),
-        lax.all_gather(up_projection_weight, "sp", axis=0, tiled=True),
+        ring_gather(up_projection_weight, "sp", 0),
         lax.all_gather(down_projection_weight, "sp", axis=1, tiled=True),
     )
     token_rows = queries.shape[0]

time: 541 us -> 508 us (0.939)
  waiting for transfers between devices: 394 us -> 342 us
  local copies, waits for them, and re-layouts: 23.3 us -> 39.3 us
    ppermute x0 -> x7, waiting for transfers between devices: none -> 174 us  [ring_gather(): x = lax.ppermute(x, axis, [(d, (d + 1) % ways) for d in range(ways)])]
    all_gather x1, waiting for transfers between devices: 84.2 us -> 0.01 us  [local(): lax.all_gather(gate_projection_weight, 'sp', axis=0, tiled=True)]
    all_gather x1 -> x0, waiting for transfers between devices: 82.7 us -> none  [local(): lax.all_gather(up_projection_weight, 'sp', axis=0, tiled=True)]
    all_gather x1, waiting for transfers between devices: 34.1 us -> 0.01 us  [local(): lax.all_gather((stream_local * scale * gain_columns).astype(jnp.bfloat16)...]
    all_gather x1, waiting for transfers between devices: 93.2 us -> 70.8 us  [local(): lax.all_gather(down_projection_weight, 'sp', axis=1, tiled=True)]
    dynamic_update_slice x0 -> x8, local copies, waits for them, and re-layouts: none -> 9.64 us  [the longest x7 8.72 us: ring_gather(): lax.dynamic_update_slice_in_dim(full, x, (here - far) % ways * step, axis...]
  transfers between devices with their start and end apart: 7 -> 13, of which waited for: 7 -> 11; matrix products, arithmetic and copies ran while one was open for 6% -> 9% of each run, Pallas kernels for 0% -> 0%
where the time goes in v1:
time: 508 us; the launch traced here: 507 us
  waiting for transfers between devices  342 us (67%)
  matrix products  53.5 us (11%)
  local copies, waits for them, and re-layouts  39.3 us (8%)
  blocking collectives  29.1 us (6%)
  other arithmetic  26.3 us (5%)
  between operations  14.3 us (3%)
    ppermute x7, waiting for transfers between devices, ring_gather(): x = lax.ppermute(x, axis, [(d, (d + 1) % ways) for d in range(ways)])  174 us
    all_gather x1, waiting for transfers between devices, local(): lax.all_gather(down_projection_weight, 'sp', axis=1, tiled=True)  70.8 us
    reduce_scatter x1, waiting for transfers between devices, local(): lax.psum_scatter(down_terms.astype(jnp.bfloat16), 'tp', scatter_dimension...  42.7 us
    reduce_scatter x1, waiting for transfers between devices, local(): lax.psum_scatter(partial_value, 'tp', scatter_dimension=1, tiled=True)  41.6 us
    unnamed x1, blocking collectives  23.3 us
    dot_general x1, matrix products, local(): down_terms = jnp.dot(hidden, whole_down, preferred_element_type=jnp.float32)  20.5 us
    all_gather x1, waiting for transfers between devices, entering(): everything = jax.tree.map(lambda part: lax.all_gather(part, axis), array)  12.5 us
    dot_general x1, matrix products, local(): gate_value = jnp.dot(normed, whole_gate, preferred_element_type=jnp.float32)  11.7 us
  transfers between devices with their start and end apart: 13, of which 11 were waited for; matrix products, arithmetic and copies ran while one was open for 9% of the time, Pallas kernels for 0%

profile of v1, /device:TPU:0, one launch (start us, length us, event | category | flops | bytes accessed | tf_op | source)
XLA Modules:
  0.0 507.3 jit_solution(16893732362691284882)
XLA Ops:
  6.6 1.4 copy.44
  8.0 1.0 copy.45
  9.0 2.3 copy.42
  11.2 2.8 convert_bitcast_fusion
  14.1 2.9 copy.43
  17.0 2.1 copy.40
  19.0 1.3 copy.41
  20.4 18.4 %while.37 = (s32[]{:T(128)}, f32[2,128,256]{2,1,0:T(8,128)S(1)}, f32[2]{0:T(128)S(1)}, f32[2]{0:T(128)S(1)}, f32[2,2,512,256]{3,2,1,0:T(8,128)}, /*index=5*/f32[...) while((s32[]{:T(128)}, f32[2,128,256]{2,1,0:T(8,128)S(1)}, ...), condition=%wide.region_5.6_spmd.clone, body=%wide.region_0.5_spmd.clone.sunk | while | flops 2557093888 | bytes 39478384 | solution.py:97
  22.8 1.5 fusion.120
  24.3 2.6 fusion.122
  27.0 1.1 fusion.123
  28.2 1.3 convolution_add_fusion.2
  32.0 1.5 fusion.120
  33.5 2.6 fusion.122
  36.2 1.1 fusion.123
  37.4 1.3 convolution_add_fusion.2
  38.8 0.7 copy-done.2
  41.2 23.3 %all-reduce.2 = (f32[16]{0:T(128)S(1)}, f32[16]{0:T(128)S(1)}) all-reduce(f32[16]{0:T(128)S(1)} %dynamic-update-slice, f32[16]{0:T(128)S(1)} %dynamic-update-slice.1), channel_id=2, replica_groups=mesh['sp'=8,'tp'=4] {'sp'}, use_global_device_ids=true, to_apply=%add | all-reduce | flops 32 | bytes 256
  64.7 4.2 copy.49
  68.9 4.1 reshape.321
  73.0 3.2 add_divide_fusion
  76.1 2.9 copy.52
  79.1 12.5 %all-gather.14.cloned.1.call-done = f32[16,128,256]{2,1,0:T(8,128)} async-done(((f32[2,128,256]{2,1,0:T(8,128)}), f32[16,128,256]{2,1,0:T(8,128)}) %all-gather.14.cloned.1.call-update) | async-done | bytes 2097168 | tf_op jit(solution)/shard_map/all_gather | solution.py:23
  91.6 9.1 %while.38 = (s32[]{:T(128)}, f32[2,128,256]{2,1,0:T(8,128)S(1)}, f32[2]{0:T(128)S(1)}, s32[]{:T(128)}, f32[8,2]{1,0:T(8,128)S(1)}, /*index=5*/f32[8,2]{1,0:T(8,1...) while((s32[]{:T(128)}, f32[2,128,256]{2,1,0:T(8,128)S(1)}, f32[2]{0:T(128)S(1)}, s32[]{:T(128)}, ...), condition=%wide.region_7.8_spmd.clone, body=%wide.region_6.7_spmd.clone.sunk | while | flops 327698 | bytes 786647 | solution.py:35
  91.6 1.1 fusion.124
  92.8 1.1 fusion.124
  93.9 1.1 fusion.124
  95.1 1.1 fusion.124
  96.2 1.1 fusion.124
  97.3 1.1 fusion.124
  98.4 1.1 fusion.124
  99.6 1.1 fusion.124
  100.8 3.9 fusion.58
  105.0 4.4 convolution_convert_fusion.1
  109.5 0.7 all-gather.10.cloned.1.call-update
  110.2 0.8 dynamic-slice_convert_fusion
  111.0 41.6 %reduce-scatter.3.cloned.1.call-done = bf16[1024,512]{1,0:T(8,128)(2,1)} async-done(((bf16[1024,2048]{1,0:T(8,128)(2,1)}), bf16[1024,512]{1,0:T(8,128)(2,1)}) %reduce-scatter.3.cloned.1.call-update) | async-done | bytes 1048592 | tf_op jit(solution)/shard_map/reduce_scatter | solution.py:190
  152.6 1.7 fusion.54
  154.3 5.8 %psum.7 = f32[1024]{0:T(1024)S(1)} all-reduce(f32[1024]{0:T(1024)S(1)} %fusion.54), channel_id=1, replica_groups=mesh['sp'=8,'tp'=4] {'tp'}, use_global_device_ids=true, to_apply=%region_11.12 | all-reduce | flops 1024 | bytes 8192 | tf_op jit(solution)/shard_map/psum | solution.py:195
  160.1 1.4 fusion.56
  162.1 1.7 collective-permute-start
  163.8 34.0 %collective-permute-done = bf16[256,1408]{1,0:T(8,128)(2,1)S(1)} collective-permute-done((bf16[256,1408]{1,0:T(8,128)(2,1)S(1)}, bf16[256,1408]{1,0:T(8,128)(2,1)S(1)}, u32[]{:S(2)}, u32[]{:S(2)}) %collective-permute-start) | collective-permute-done | bytes 720928 | tf_op jit(solution)/shard_map/ppermute | solution.py:16
  197.8 27.2 %collective-permute-done.1 = bf16[256,1408]{1,0:T(8,128)(2,1)S(1)} collective-permute-done((bf16[256,1408]{1,0:T(8,128)(2,1)S(1)}, bf16[256,1408]{1,0:T(8,128)(2,1)S(1)}, u32[]{:S(2)}, u32[]{:S(2)}) %collective-permute-start.1) | collective-permute-done | bytes 720928 | tf_op jit(solution)/shard_map/ppermute | solution.py:16
  225.0 0.9 copy-done.13
  225.9 36.5 %collective-permute-done.2 = bf16[256,1408]{1,0:T(8,128)(2,1)S(1)} collective-permute-done((bf16[256,1408]{1,0:T(8,128)(2,1)S(1)}, bf16[256,1408]{1,0:T(8,128)(2,1)S(1)}, u32[]{:S(2)}, u32[]{:S(2)}) %collective-permute-start.2) | collective-permute-done | bytes 720928 | tf_op jit(solution)/shard_map/ppermute | solution.py:16
  262.4 0.9 copy-done.15
  263.3 37.2 %collective-permute-done.3 = bf16[256,1408]{1,0:T(8,128)(2,1)} collective-permute-done((bf16[256,1408]{1,0:T(8,128)(2,1)S(1)}, bf16[256,1408]{1,0:T(8,128)(2,1)}, u32[]{:S(2)}, u32[]{:S(2)}) %collective-permute-start.3) | collective-permute-done | bytes 720928 | tf_op jit(solution)/shard_map/ppermute | solution.py:16
  300.5 2.9 broadcast_in_dim.38
  303.5 0.9 constant_dynamic-update-slice_fusion.7
  304.4 10.5 %collective-permute-done.4 = bf16[256,1408]{1,0:T(8,128)(2,1)} collective-permute-done((bf16[256,1408]{1,0:T(8,128)(2,1)}, bf16[256,1408]{1,0:T(8,128)(2,1)}, u32[]{:S(2)}, u32[]{:S(2)}) %collective-permute-start.4) | collective-permute-done | bytes 720928 | tf_op jit(solution)/shard_map/ppermute | solution.py:16
  314.8 0.9 constant_dynamic-update-slice_fusion.6
  315.8 0.9 constant_dynamic-update-slice_fusion.5
  316.7 0.9 constant_dynamic-update-slice_fusion.4
  317.7 15.7 %collective-permute-done.5 = bf16[256,1408]{1,0:T(8,128)(2,1)S(1)} collective-permute-done((bf16[256,1408]{1,0:T(8,128)(2,1)}, bf16[256,1408]{1,0:T(8,128)(2,1)S(1)}, u32[]{:S(2)}, u32[]{:S(2)}) %collective-permute-start.5) | collective-permute-done | bytes 720928 | tf_op jit(solution)/shard_map/ppermute | solution.py:16
  333.4 2.0 constant_dynamic-update-slice_fusion.3
  335.4 2.1 constant_dynamic-update-slice_fusion.2
  337.5 0.9 constant_dynamic-update-slice_fusion.1
  338.4 12.4 %collective-permute-done.6 = bf16[256,1408]{1,0:T(8,128)(2,1)S(1)} collective-permute-done((bf16[256,1408]{1,0:T(8,128)(2,1)S(1)}, bf16[256,1408]{1,0:T(8,128)(2,1)S(1)}, u32[]{:S(2)}, u32[]{:S(2)}) %collective-permute-start.6) | collective-permute-done | bytes 720928 | tf_op jit(solution)/shard_map/ppermute | solution.py:16
  350.8 0.9 constant_dynamic-update-slice_fusion
  351.7 11.7 %fusion.74 = f32[1024,1408]{1,0:T(8,128)} fusion(bf16[1024,2048]{1,0:T(8,128)(2,1)} %all-gather.8.cloned.1.call-done, bf16[2048,1408]{1,0:T(8,128)(2,1)} %all-gather.10.cloned.1.call-done), kind=kOutput, calls=%fused_computation.125 | convolution fusion | flops 5905580032 | bytes 15728640 | tf_op jit(solution)/shard_map/dot_general | solution.py:203
  363.4 70.8 %all-gather.12.cloned.1.call-done = bf16[1408,2048]{1,0:T(8,128)(2,1)} async-done(((bf16[1408,256]{1,0:T(8,128)(2,1)}), bf16[1408,2048]{1,0:T(8,128)(2,1)}) %all-gather.12.cloned.1.call-update) | async-done | bytes 5767184 | tf_op jit(solution)/shard_map/all_gather | solution.py:136
  434.2 20.5 %convolution_convert_fusion = bf16[1024,2048]{1,0:T(8,128)(2,1)} fusion(bf16[1408,2048]{1,0:T(8,128)(2,1)} %all-gather.12.cloned.1.call-done, f32[1024,1408]{1,0:T(8,128)} %fusion.74, bf16[1024,2048]{1,0:T(8,128)(2,1)} %all-gather.8.cloned.1.call-done, bf16[2048,1408]{1,0:T(8,128)(2,1)} %constant_dynamic-update-slice_fusion), kind=kOutput, calls=%fused_computation.80 | convolution fusion | flops 11821907968 | bytes 25690112 | tf_op jit(solution)/shard_map/dot_general | solution.py:206
  454.8 42.7 %reduce-scatter.5.cloned.1.call-done = bf16[1024,512]{1,0:T(8,128)(2,1)} async-done(((bf16[1024,2048]{1,0:T(8,128)(2,1)}), bf16[1024,512]{1,0:T(8,128)(2,1)}) %reduce-scatter.5.cloned.1.call-update) | async-done | bytes 1048592 | tf_op jit(solution)/shard_map/reduce_scatter | solution.py:207
  497.5 3.0 fusion.57
  (142 shorter events, 8.0 us)
Async XLA Ops:
  6.5 98.5 %copy-start = (bf16[512,2048]{1,0:T(8,128)(2,1)S(1)}, bf16[512,2048]{1,0:T(8,128)(2,1)}, u32[]{:S(2)}) copy-start(bf16[512,2048]{1,0:T(8,128)(2,1)} %param.27) | copy-start | bytes 6291460
  6.5 85.0 %all-gather.14.cloned.1.call-start = ((), (), s32[]{:S(2)}) async-start(), calls=%async_computation.7 | async-start | bytes 2359296 | tf_op jit(solution)/shard_map/all_gather | solution.py:23
  8.0 6.1 %copy-start.8 = (bf16[1024,256]{0,1:T(8,128)(2,1)}, bf16[1024,256]{0,1:T(8,128)(2,1)S(1)}, u32[]{:S(2)}) copy-start(bf16[1024,256]{0,1:T(8,128)(2,1)S(1)} %copy.44) | copy-start | bytes 1572868
  16.9 3.4 copy-start.18
  16.9 3.4 copy-start.17
  16.9 3.4 copy-start.19
  20.4 19.2 %copy-start.21 = (u32[32]{0:T(128)S(1)}, u32[32]{0:T(128)}, u32[]{:S(2)}) copy-start(u32[32]{0:T(128)} %constant.161) | copy-start | bytes 388
  22.7 1.7 copy-start.3
  24.3 2.7 copy-start.4
  24.3 2.7 copy-start.10
  28.1 1.4 copy-start.11
  31.8 1.7 copy-start.3
  33.5 2.7 copy-start.4
  33.5 2.7 copy-start.10
  37.3 1.4 copy-start.11
  38.8 0.7 copy-start.2
  39.6 113.0 %reduce-scatter.3.cloned.1.call-start = ((), (), s32[]{:S(2)}) async-start(), calls=%async_computation.2 | async-start | bytes 5242880 | tf_op jit(solution)/shard_map/reduce_scatter | solution.py:190
  76.1 2.9 copy-start.20
  91.6 9.2 %copy-start.9 = (bf16[1024,256]{0,1:T(8,128)(2,1)S(1)}, bf16[1024,256]{0,1:T(8,128)(2,1)}, u32[]{:S(2)}) copy-start(bf16[1024,256]{0,1:T(8,128)(2,1)} %copy-done.8) | copy-start | bytes 1572868
  100.8 3.9 copy-start.7
  109.4 43.1 %copy-start.5 = (bf16[1024,512]{1,0:T(8,128)(2,1)S(1)}, bf16[1024,512]{1,0:T(8,128)(2,1)}, u32[]{:S(2)}) copy-start(bf16[1024,512]{1,0:T(8,128)(2,1)} %param.25) | copy-start | bytes 3145732
  109.5 242.3 %all-gather.10.cloned.1.call-start = ((), (), s32[]{:S(2)}) async-start(), calls=%async_computation.4 | async-start | bytes 6488064 | tf_op jit(solution)/shard_map/all_gather | solution.py:134
  110.2 241.5 %all-gather.8.cloned.1.call-start = ((), (), s32[]{:S(2)}) async-start(), calls=%async_computation.3 | async-start | bytes 5242880 | tf_op jit(solution)/shard_map/all_gather | solution.py:200
  152.6 7.5 %copy-start.6 = (bf16[1024,512]{1,0:T(8,128)(2,1)S(1)}, bf16[1024,512]{1,0:T(8,128)(2,1)}, u32[]{:S(2)}) copy-start(bf16[1024,512]{1,0:T(8,128)(2,1)} %reduce-scatter.3.cloned.1.call-done) | copy-start | bytes 3145732
  160.1 2.0 copy-start.12
  161.5 272.7 %all-gather.12.cloned.1.call-start = ((), (), s32[]{:S(2)}) async-start(), calls=%async_computation.5 | async-start | bytes 6488064 | tf_op jit(solution)/shard_map/all_gather | solution.py:136
  162.1 335.4 %reduce-scatter.5.cloned.1.call-start = ((), (), s32[]{:S(2)}) async-start(), calls=%async_computation.6 | async-start | bytes 5242880 | tf_op jit(solution)/shard_map/reduce_scatter | solution.py:207
  162.1 35.7 %collective-permute-start = (bf16[256,1408]{1,0:T(8,128)(2,1)S(1)}, bf16[256,1408]{1,0:T(8,128)(2,1)S(1)}, u32[]{:S(2)}, u32[]{:S(2)}) collective-permute-start(bf16[256,1408]{1,0:T(8,128)(2,1)S(1)} %copy-done.12), channel_id=1, source_target_pairs={{0,4},{4,8},{8,12},{12,16},{16,20},{20,24},{24,28},{28,0},{1,5},{5... | collective-permute-start | bytes 2162696 | tf_op jit(solution)/shard_map/ppermute | solution.py:16
  197.8 27.2 %collective-permute-start.1 = (bf16[256,1408]{1,0:T(8,128)(2,1)S(1)}, bf16[256,1408]{1,0:T(8,128)(2,1)S(1)}, u32[]{:S(2)}, u32[]{:S(2)}) collective-permute-start(bf16[256,1408]{1,0:T(8,128)(2,1)S(1)} %collective-permute-done), channel_id=1, source_target_pairs={{0,4},{4,8},{8,12},{12,16},{16,20},{20,24},{24,28},{28,0},{1,5},{5... | collective-permute-start | bytes 2162696 | tf_op jit(solution)/shard_map/ppermute | solution.py:16
  225.0 0.9 copy-start.13
  225.9 36.5 %collective-permute-start.2 = (bf16[256,1408]{1,0:T(8,128)(2,1)S(1)}, bf16[256,1408]{1,0:T(8,128)(2,1)S(1)}, u32[]{:S(2)}, u32[]{:S(2)}) collective-permute-start(bf16[256,1408]{1,0:T(8,128)(2,1)S(1)} %collective-permute-done.1), channel_id=1, source_target_pairs={{0,4},{4,8},{8,12},{12,16},{16,20},{20,24},{24,28},{28,0},{1,5},{5... | collective-permute-start | bytes 2162696 | tf_op jit(solution)/shard_map/ppermute | solution.py:16
  262.4 0.9 copy-start.15
  263.3 37.3 %collective-permute-start.3 = (bf16[256,1408]{1,0:T(8,128)(2,1)S(1)}, bf16[256,1408]{1,0:T(8,128)(2,1)}, u32[]{:S(2)}, u32[]{:S(2)}) collective-permute-start(bf16[256,1408]{1,0:T(8,128)(2,1)S(1)} %collective-permute-done.2), channel_id=1, source_target_pairs={{0,4},{4,8},{8,12},{12,16},{16,20},{20,24},{24,28},{28,0},{1,5},{5... | collective-permute-start | bytes 2162696 | tf_op jit(solution)/shard_map/ppermute | solution.py:16
  300.5 14.3 %collective-permute-start.4 = (bf16[256,1408]{1,0:T(8,128)(2,1)}, bf16[256,1408]{1,0:T(8,128)(2,1)}, u32[]{:S(2)}, u32[]{:S(2)}) collective-permute-start(bf16[256,1408]{1,0:T(8,128)(2,1)} %collective-permute-done.3), channel_id=1, source_target_pairs={{0,4},{4,8},{8,12},{12,16},{16,20},{20,24},{24,28},{28,0},{1,5},{5... | collective-permute-start | bytes 2162696 | tf_op jit(solution)/shard_map/ppermute | solution.py:16
  303.4 12.3 %copy-start.14 = (bf16[256,1408]{1,0:T(8,128)(2,1)S(1)}, bf16[256,1408]{1,0:T(8,128)(2,1)}, u32[]{:S(2)}) copy-start(bf16[256,1408]{1,0:T(8,128)(2,1)} %copy-done.13) | copy-start | bytes 2162692
  303.4 13.3 %copy-start.16 = (bf16[256,1408]{1,0:T(8,128)(2,1)S(1)}, bf16[256,1408]{1,0:T(8,128)(2,1)}, u32[]{:S(2)}) copy-start(bf16[256,1408]{1,0:T(8,128)(2,1)} %copy-done.15) | copy-start | bytes 2162692
  314.8 18.5 %collective-permute-start.5 = (bf16[256,1408]{1,0:T(8,128)(2,1)}, bf16[256,1408]{1,0:T(8,128)(2,1)S(1)}, u32[]{:S(2)}, u32[]{:S(2)}) collective-permute-start(bf16[256,1408]{1,0:T(8,128)(2,1)} %collective-permute-done.4), channel_id=1, source_target_pairs={{0,4},{4,8},{8,12},{12,16},{16,20},{20,24},{24,28},{28,0},{1,5},{5... | collective-permute-start | bytes 2162696 | tf_op jit(solution)/shard_map/ppermute | solution.py:16
  333.4 17.5 %collective-permute-start.6 = (bf16[256,1408]{1,0:T(8,128)(2,1)S(1)}, bf16[256,1408]{1,0:T(8,128)(2,1)S(1)}, u32[]{:S(2)}, u32[]{:S(2)}) collective-permute-start(bf16[256,1408]{1,0:T(8,128)(2,1)S(1)} %collective-permute-done.5), channel_id=1, source_target_pairs={{0,4},{4,8},{8,12},{12,16},{16,20},{20,24},{24,28},{28,0},{1,5},{5... | collective-permute-start | bytes 2162696 | tf_op jit(solution)/shard_map/ppermute | solution.py:16
  454.8 45.7 %copy-start.1 = (bf16[512,2048]{1,0:T(8,128)(2,1)S(1)}, bf16[512,2048]{1,0:T(8,128)(2,1)}, u32[]{:S(2)}) copy-start(bf16[512,2048]{1,0:T(8,128)(2,1)} %param.27) | copy-start | bytes 6291460
Sparse Core Ops, SparseCore 0:
  39.7 51.8 all-gather.13
  109.6 42.9 reduce-scatter.2
  154.7 130.4 all-gather.9
  286.6 52.4 all-gather.7
  341.0 93.1 all-gather.11
  454.9 42.5 reduce-scatter.4
